TPU v7x, 32 devices: a whole 2x2x4 slice. The times are simulated.
32 devices in a mesh: grp: 2 (over y), sp: 4 (over z), tp: 4 (over x, core).
Axes of the slice: x: 2, y: 2, z: 4, core: 2. Of those that a mesh axis runs over, the one named last changes fastest.
Arguments:
- residual: bfloat16 [2048, 2048], P(('grp', 'sp', 'tp')), parts along dimension 0, may hold values from -6 to 6
- queries_wide: bfloat16 [2048, 1024], P(('grp', 'sp'), 'tp'), parts along dimension 0, may hold values from -6 to 6
- keys_wide: bfloat16 [2048, 512], P(('grp', 'sp'), 'tp'), parts along dimension 0, may hold values from -6 to 6
- values_wide: bfloat16 [2048, 512], P(('grp', 'sp'), 'tp'), parts along dimension 0, may hold values from -6 to 6
- queries_narrow: bfloat16 [2048, 512], P(('grp', 'sp'), 'tp'), parts along dimension 0, may hold values from -6 to 6
- keys_narrow: bfloat16 [2048, 256], P(('grp', 'sp'), 'tp'), parts along dimension 0, may hold values from -6 to 6
- values_narrow: bfloat16 [2048, 256], P(('grp', 'sp'), 'tp'), parts along dimension 0, may hold values from -6 to 6
- query_gain_wide: float32 [128], replicated, may hold values from 1 to 6
- key_gain_wide: float32 [128], replicated, may hold values from 1 to 6
- query_gain_narrow: float32 [64], replicated, may hold values from 1 to 6
- key_gain_narrow: float32 [64], replicated, may hold values from 1 to 6
- output_wide: bfloat16 [1024, 2048], P('tp'), may hold values from -0.3125 to 0.3125
- output_narrow: bfloat16 [512, 2048], P('tp'), may hold values from -0.3125 to 0.3125
- norm_gain: float32 [2048], replicated, may hold values from 0.1 to 1.9
- gate_weight: bfloat16 [4, 2048, 3584], P('sp', None, 'tp'), may hold values from -0.125 to 0.125
- up_weight: bfloat16 [4, 2048, 3584], P('sp', None, 'tp'), may hold values from -0.125 to 0.125
- down_weight: bfloat16 [4, 3584, 2048], P('sp', 'tp'), may hold values from -0.09375 to 0.09375
- route_ids: int32 [2048, 2], P(('grp', 'sp', 'tp')), parts along dimension 0, may hold values from 0 to 3, all different within a row; in each aligned block of 64 rows (0 to 63, 64 to 127, ...) at most 64 rows name the same one
- route_weights: float32 [2048, 2], P(('grp', 'sp', 'tp')), parts along dimension 0, may hold values from 0.1 to 0.9
Outputs:
- result: bfloat16 [2048, 2048], P(('grp', 'sp', 'tp')), parts along dimension 0
There are 2 independent parts, one for each index of `grp`. A program takes and returns all parts, laid end to end along the dimension named above; an argument that names none is the same for every part. Nothing has to cross between parts.
Inputs may be any that keep to these rules, and one draw needn't show every extreme that they name: `route_ids`: in each aligned block of 64 rows (the rows of one device) no expert is named by more than 64 rows, a bound that some block reaches; a row names 2 different experts.
All inputs are finite; a program needn't handle non-finite values.
Results may differ from a plain program's by a relative error of at most 0.013.
The roundings to bfloat16 on the way count: a program that leaves them out, or rounds other values in their place, can miss the bound.
Values may be sent and summed in bfloat16 or wider, within the bound.
A program may use at most 128 MiB of HBM per device.

v0:
```python
import functools

import jax
import jax.numpy as jnp
import numpy as np
from jax import lax
from jax.experimental import pallas as pl
from jax.experimental.pallas import tpu as pltpu
from jax.sharding import PartitionSpec as P

GRID = 64


THETA = 10000.0
EPS = 1e-06
NEG_BIG = -1e30


def rotary_tables(places, head_width):
    quarter = head_width // 4
    inv_freq = THETA ** (-jnp.arange(quarter, dtype=jnp.float32) / quarter)
    grid_rows = (places // GRID).astype(jnp.float32)
    grid_cols = (places % GRID).astype(jnp.float32)
    row_angle = grid_rows[:, None] * inv_freq[None, :]
    col_angle = grid_cols[:, None] * inv_freq[None, :]
    angles = jnp.concatenate([row_angle, row_angle, col_angle, col_angle], axis=-1)
    return (jnp.cos(angles), jnp.sin(angles))


def head_norm_rotate(values, gain_vec, cos_table, sin_table):
    as_float = values.astype(jnp.float32)
    scaled = as_float * lax.rsqrt(jnp.mean(as_float * as_float, axis=-1, keepdims=True) + EPS)
    scaled = scaled * gain_vec
    full_shape = scaled.shape
    quarter = full_shape[-1] // 4
    halves = scaled.reshape(full_shape[:-1] + (2, 2, quarter))
    turned = jnp.stack([-halves[..., 1, :], halves[..., 0, :]], axis=-2).reshape(full_shape)
    return (scaled * cos_table[:, None, :] + turned * sin_table[:, None, :]).astype(jnp.bfloat16)


def fresh_state(queries):
    key_heads, group_size, tok_count = (queries.shape[1], queries.shape[2], queries.shape[0])
    return (
        jnp.full((key_heads, group_size, tok_count), NEG_BIG, jnp.float32),
        jnp.zeros((key_heads, group_size, tok_count), jnp.float32),
        jnp.zeros(queries.shape, jnp.float32),
    )


def key_sweep(carried, queries, keys, values):
    key_count = keys.shape[0]
    key_heads = queries.shape[1]
    head_width = queries.shape[3]
    block_len = 2048 if key_count % 2048 == 0 else key_count
    key_blocks = keys.reshape(key_count // block_len, block_len, key_heads, head_width)
    value_blocks = values.reshape(key_count // block_len, block_len, key_heads, head_width)
    score_scale = head_width ** (-0.5)

    def step(carried_state, blocks_in):
        key_block, value_block = blocks_in
        running_max, weight_sum, weighted = carried_state
        scores = (
            jnp.einsum("qhgd,khd->hgqk", queries, key_block, preferred_element_type=jnp.float32)
            * score_scale
        )
        new_max = jnp.maximum(running_max, jnp.max(scores, axis=-1))
        weights = jnp.exp(scores - new_max[..., None])
        rescale = jnp.exp(running_max - new_max)
        weight_sum = weight_sum * rescale + jnp.sum(weights, axis=-1)
        mixed_values = jnp.einsum(
            "hgqk,khd->qhgd",
            weights.astype(jnp.bfloat16),
            value_block,
            preferred_element_type=jnp.float32,
        )
        weighted = weighted * jnp.transpose(rescale, (2, 0, 1))[..., None] + mixed_values
        return ((new_max, weight_sum, weighted), None)

    carried, _ = lax.scan(step, carried, (key_blocks, value_blocks))
    return carried


def finish_heads(carried):
    weighted = carried[2]
    outcome = weighted / jnp.transpose(carried[1], (2, 0, 1))[..., None]
    return outcome.astype(jnp.bfloat16).reshape(weighted.shape[0], -1)


def slot_tables(chosen, slot_count, expert_count):
    row_count = chosen.shape[0]
    pick_count = chosen.shape[1]
    flat_pick = chosen.reshape(row_count * pick_count)
    hit_marks = (flat_pick[:, None] == jnp.arange(expert_count, dtype=jnp.int32)[None, :]).astype(
        jnp.int32
    )
    before = jnp.cumsum(hit_marks, axis=0) - hit_marks
    slot_place = jnp.sum(before * hit_marks, axis=1)
    target = flat_pick * slot_count + slot_place
    slot_table = target[:, None] == jnp.arange(expert_count * slot_count, dtype=jnp.int32)[None, :]
    return slot_table.astype(jnp.bfloat16).reshape(row_count, pick_count, expert_count * slot_count)


def plain_body(
    residual,
    queries_wide,
    keys_wide,
    values_wide,
    queries_narrow,
    keys_narrow,
    values_narrow,
    query_gain_wide,
    key_gain_wide,
    query_gain_narrow,
    key_gain_narrow,
    output_wide,
    output_narrow,
    norm_gain,
    gate_weight,
    up_weight,
    down_weight,
    route_ids,
    route_weights,
):
    tok_count = queries_wide.shape[0]
    places = lax.axis_index("sp") * tok_count + jnp.arange(tok_count, dtype=jnp.int32)
    wide_width = query_gain_wide.shape[0]
    narrow_width = query_gain_narrow.shape[0]
    cos_wide, sin_wide = rotary_tables(places, wide_width)
    cos_narrow, sin_narrow = rotary_tables(places, narrow_width)
    wide_keyheads = keys_wide.shape[1] // wide_width
    narrow_keyheads = keys_narrow.shape[1] // narrow_width
    q_wide = head_norm_rotate(
        queries_wide.reshape(tok_count, -1, wide_width), query_gain_wide, cos_wide, sin_wide
    )
    q_wide = q_wide.reshape(tok_count, wide_keyheads, -1, wide_width)
    k_wide = head_norm_rotate(
        keys_wide.reshape(tok_count, -1, wide_width), key_gain_wide, cos_wide, sin_wide
    )
    k_wide = k_wide.reshape(tok_count, -1)
    q_narrow = head_norm_rotate(
        queries_narrow.reshape(tok_count, -1, narrow_width),
        query_gain_narrow,
        cos_narrow,
        sin_narrow,
    )
    q_narrow = q_narrow.reshape(tok_count, narrow_keyheads, -1, narrow_width)
    k_narrow = head_norm_rotate(
        keys_narrow.reshape(tok_count, -1, narrow_width), key_gain_narrow, cos_narrow, sin_narrow
    )
    k_narrow = k_narrow.reshape(tok_count, -1)
    carried = (fresh_state(q_wide), fresh_state(q_narrow))
    carried = (
        key_sweep(
            carried[0],
            q_wide,
            lax.all_gather(k_wide, "sp", axis=0, tiled=True),
            lax.all_gather(values_wide, "sp", axis=0, tiled=True),
        ),
        key_sweep(
            carried[1],
            q_narrow,
            lax.all_gather(k_narrow, "sp", axis=0, tiled=True),
            lax.all_gather(values_narrow, "sp", axis=0, tiled=True),
        ),
    )
    heads_wide = finish_heads(carried[0])
    heads_narrow = finish_heads(carried[1])
    own_rows = residual.shape[0]
    mixed_heads = lax.psum_scatter(
        (
            jnp.dot(heads_wide, output_wide, preferred_element_type=jnp.float32)
            + jnp.dot(heads_narrow, output_narrow, preferred_element_type=jnp.float32)
        ).astype(jnp.bfloat16),
        "tp",
        scatter_dimension=0,
        tiled=True,
    ).astype(jnp.float32)
    attended = (residual.astype(jnp.float32) + mixed_heads).astype(jnp.bfloat16)
    state_float = attended.astype(jnp.float32)
    normed = (
        state_float
        * lax.rsqrt(jnp.mean(state_float * state_float, axis=-1, keepdims=True) + EPS)
        * norm_gain
    ).astype(jnp.bfloat16)
    pick_count = route_ids.shape[1]
    expert_count = lax.axis_size("sp")
    slot_count = 2 * pick_count * own_rows // expert_count
    model_width = residual.shape[1]
    own_tables = slot_tables(route_ids, slot_count, expert_count)
    send_rows = jnp.einsum(
        "rks,rd->sd", own_tables, normed, preferred_element_type=jnp.float32
    ).astype(jnp.bfloat16)
    send_rows = send_rows.reshape(expert_count, slot_count, model_width)
    arrived = lax.all_to_all(send_rows, "sp", split_axis=0, concat_axis=0, tiled=True)
    copies = lax.all_gather(arrived, "tp", axis=0, tiled=True)
    expert_arrived = copies.reshape((lax.axis_size("tp"),) + arrived.shape)
    full_shape = expert_arrived.shape
    flat_rows = expert_arrived.reshape(-1, model_width)
    gate_act = jnp.dot(flat_rows, gate_weight[0], preferred_element_type=jnp.float32)
    up_act = jnp.dot(flat_rows, up_weight[0], preferred_element_type=jnp.float32)
    hidden = (jax.nn.silu(gate_act) * up_act).astype(jnp.bfloat16)
    partial_value = jnp.dot(hidden, down_weight[0], preferred_element_type=jnp.float32).reshape(
        full_shape
    )
    summed = lax.psum_scatter(
        partial_value.astype(jnp.bfloat16), "tp", scatter_dimension=0, tiled=True
    ).astype(jnp.float32)
    results = summed.reshape(full_shape[1:]).astype(jnp.bfloat16)
    returned = lax.all_to_all(results, "sp", split_axis=0, concat_axis=0, tiled=True)
    returned_flat = returned.reshape(expert_count * slot_count, model_width)
    picked = jnp.einsum(
        "rks,sd->rkd", own_tables, returned_flat, preferred_element_type=jnp.float32
    )
    mixture = jnp.sum(route_weights[:, :, None] * picked, axis=1)
    return (state_float + mixture).astype(jnp.bfloat16)


LANES = 128
MESH_IDS = pl.DeviceIdType.MESH


def pick(table, row, col):
    found = jnp.int32(0)
    for a in range(len(table)):
        for b in range(len(table[0])):
            found = jnp.where((row == a) & (col == b), jnp.int32(table[a][b]), found)
    return found


def remote(src, dst, send_sem, recv_sem, target):
    return pltpu.make_async_remote_copy(
        src_ref=src,
        dst_ref=dst,
        send_sem=send_sem,
        recv_sem=recv_sem,
        device_id=target,
        device_id_type=MESH_IDS,
    )


def lane_index(shape):
    return lax.broadcasted_iota(jnp.int32, shape, len(shape) - 1)


def turn_rotate(scaled, cos_table, sin_signed, quarter):
    lane = lane_index(scaled.shape)
    ahead = pltpu.roll(scaled, LANES - quarter, 1)
    behind = pltpu.roll(scaled, quarter, 1)
    return scaled * cos_table + jnp.where(lane % (2 * quarter) < quarter, ahead, behind) * sin_signed


def rotate_full(values, gain, cos_table, sin_signed):
    scaled = values * lax.rsqrt(jnp.mean(values * values, axis=-1, keepdims=True) + EPS) * gain
    return turn_rotate(scaled, cos_table, sin_signed, LANES // 4)


def rotate_half(values, gain, cos_table, sin_signed):
    half = LANES // 2
    low = lane_index(values.shape) < half
    square = values * values
    mean_low = jnp.sum(jnp.where(low, square, 0.0), axis=-1, keepdims=True) / half
    mean_high = jnp.sum(jnp.where(low, 0.0, square), axis=-1, keepdims=True) / half
    scaled = values * lax.rsqrt(jnp.where(low, mean_low, mean_high) + EPS) * gain
    return turn_rotate(scaled, cos_table, sin_signed, half // 4)


def fused_kernel(
    n_sp,
    n_tp,
    residual,
    queries_wide,
    keys_wide,
    values_wide,
    queries_narrow,
    keys_narrow,
    values_narrow,
    all_tables,
    query_gain_wide,
    key_gain_wide,
    query_gain_narrow,
    key_gain_narrow,
    norm_gain,
    routed,
    output_wide,
    output_narrow,
    gate_weight,
    up_weight,
    down_weight,
    result,
    kv,
    q_wide,
    q_narrow,
    top,
    total,
    mixed,
    heads,
    out_rows,
    term,
    term_in,
    term_sum,
    term_cross,
    attended,
    rows_all,
    gate_up,
    down,
    hidden,
    part,
    pair_in,
    pair_sum,
    cross_in,
    chain_out,
    chain_in,
    final,
    tables,
    load_sem,
    kv_send,
    kv_recv,
    tp_send,
    tp_recv,
    ag_send,
    ag_recv,
    pair_send,
    pair_recv,
    cross_send,
    cross_recv,
    chain_send,
    chain_recv,
):
    me_s = lax.axis_index("sp")
    me_t = lax.axis_index("tp")
    core = me_t % 2
    column = me_t // 2
    partner = column * 2 + (1 - core)
    across = (1 - column) * 2 + core
    diagonal = (1 - column) * 2 + (1 - core)
    to_partner, to_across = {"tp": partner}, {"tp": across}
    has_left, has_right = me_s > 0, me_s < n_sp - 1
    to_left, to_right = {"sp": jnp.maximum(me_s - 1, 0)}, {"sp": jnp.minimum(me_s + 1, n_sp - 1)}
    near = [sorted(range(n_sp), key=lambda z: (abs(z - s), z)) for s in range(n_sp)]
    far = [order[::-1] for order in near]
    own = residual.shape[0]
    width = residual.shape[1]
    toks = queries_wide.shape[0]
    group = n_tp * own
    half = width // 2

    chunks = gate_weight.shape[2] // LANES
    table_load = pltpu.make_async_copy(
        all_tables.at[:, me_s], tables, load_sem.at[3 + 2 * chunks]
    )
    table_load.start()
    loads = [
        pltpu.make_async_copy(output_wide, out_rows.at[pl.ds(0, 2 * LANES)], load_sem.at[0]),
        pltpu.make_async_copy(output_narrow, out_rows.at[pl.ds(2 * LANES, LANES)], load_sem.at[1]),
        pltpu.make_async_copy(down_weight.at[0], down, load_sem.at[2]),
    ]
    for j in range(chunks):
        source = pl.ds(j * LANES, LANES)
        loads.append(
            pltpu.make_async_copy(
                gate_weight.at[0, :, source],
                gate_up.at[:, pl.ds(2 * j * LANES, LANES)],
                load_sem.at[3 + 2 * j],
            )
        )
        loads.append(
            pltpu.make_async_copy(
                up_weight.at[0, :, source],
                gate_up.at[:, pl.ds((2 * j + 1) * LANES, LANES)],
                load_sem.at[4 + 2 * j],
            )
        )
    barrier = pltpu.get_barrier_semaphore()
    pl.semaphore_signal(barrier, inc=1, device_id=to_partner, device_id_type=MESH_IDS)
    pl.semaphore_signal(barrier, inc=1, device_id=to_across, device_id_type=MESH_IDS)

    @pl.when(has_left)
    def _():
        pl.semaphore_signal(barrier, inc=1, device_id=to_left, device_id_type=MESH_IDS)

    @pl.when(has_right)
    def _():
        pl.semaphore_signal(barrier, inc=1, device_id=to_right, device_id_type=MESH_IDS)

    table_load.wait()
    for load in loads:
        load.start()
    cos_wide, sin_wide = tables[0], tables[1]
    cos_narrow, sin_narrow = tables[2], tables[3]
    low = lane_index((toks, LANES)) < LANES // 2
    key_rot = rotate_full(keys_wide[...].astype(jnp.float32), key_gain_wide[...], cos_wide, sin_wide)
    kv[me_s, :, 0:LANES] = key_rot.astype(jnp.bfloat16)
    kv[me_s, :, LANES : 2 * LANES] = values_wide[...]
    packed = jnp.concatenate(
        [keys_narrow[...].astype(jnp.float32), values_narrow[...].astype(jnp.float32)], axis=0
    ).T
    packed_rot = rotate_half(packed, jnp.concatenate([key_gain_narrow[...]] * 2, axis=1), cos_narrow, sin_narrow)
    kv[me_s, :, 2 * LANES : 3 * LANES] = jnp.where(low, packed_rot, packed).astype(jnp.bfloat16)

    greeted = 2 + jnp.where(has_left, 1, 0) + jnp.where(has_right, 1, 0)
    pl.semaphore_wait(barrier, greeted)

    def kv_copy(block, way, target):
        return remote(kv.at[block], kv.at[block], kv_send.at[way, block], kv_recv.at[block], target)

    @pl.when(has_right)
    def _():
        kv_copy(me_s, 0, to_right).start()

    @pl.when(has_left)
    def _():
        kv_copy(me_s, 1, to_left).start()

    for h in range(2):
        turned = rotate_full(
            queries_wide[:, h * LANES : (h + 1) * LANES].astype(jnp.float32),
            query_gain_wide[...],
            cos_wide,
            sin_wide,
        )
        q_wide[h * toks : (h + 1) * toks, :] = turned.astype(jnp.bfloat16)
    turned = rotate_half(
        queries_narrow[...].astype(jnp.float32), jnp.concatenate([query_gain_narrow[...]] * 2, axis=1), cos_narrow, sin_narrow
    )
    q_narrow[0:toks, :] = jnp.where(low, turned, 0.0).astype(jnp.bfloat16)
    q_narrow[toks : 2 * toks, :] = jnp.where(
        low, pltpu.roll(turned, LANES // 2, 1), 0.0
    ).astype(jnp.bfloat16)
    top[...] = jnp.full(top.shape, NEG_BIG, jnp.float32)
    total[...] = jnp.zeros(total.shape, jnp.float32)
    mixed[...] = jnp.zeros(mixed.shape, jnp.float32)

    def sweep(kind, queries, keys, values, scale):
        scores = lax.dot_general(
            queries, keys, (((1,), (1,)), ((), ())), preferred_element_type=jnp.float32
        )
        old_top = top[kind]
        new_top = jnp.maximum(old_top, jnp.max(scores, axis=-1, keepdims=True))
        weights = jnp.exp((scores - new_top) * scale)
        rescale = jnp.exp((old_top - new_top) * scale)
        total[kind] = total[kind] * rescale + jnp.sum(weights, axis=-1, keepdims=True)
        mixed[kind] = mixed[kind] * rescale + jnp.dot(
            weights.astype(jnp.bfloat16), values, preferred_element_type=jnp.float32
        )
        top[kind] = new_top

    def attend_step(i, carry):
        block = pick(near, me_s, i)
        sweep(
            0,
            q_wide[...],
            kv[block, :, 0:LANES],
            kv[block, :, LANES : 2 * LANES],
            LANES**-0.5,
        )
        both = kv[block, :, 2 * LANES : 3 * LANES]
        sweep(1, q_narrow[...], both, both, (LANES // 2) ** -0.5)
        lower, upper = me_s - (i + 1), me_s + (i + 1)

        @pl.when(lower >= 0)
        def _():
            kv_copy(lower, 0, to_right).wait_recv()

            @pl.when(has_right)
            def _():
                kv_copy(lower, 0, to_right).start()

        @pl.when(upper < n_sp)
        def _():
            kv_copy(upper, 1, to_left).wait_recv()

            @pl.when(has_left)
            def _():
                kv_copy(upper, 1, to_left).start()

        return carry

    lax.fori_loop(0, n_sp, attend_step, 0)

    head_wide = mixed[0] / total[0]
    head_narrow = mixed[1] / total[1]
    heads[:, 0:LANES] = head_wide[0:toks].astype(jnp.bfloat16)
    heads[:, LANES : 2 * LANES] = head_wide[toks : 2 * toks].astype(jnp.bfloat16)
    heads[:, 2 * LANES : 3 * LANES] = jnp.where(
        low, pltpu.roll(head_narrow[0:toks], LANES // 2, 1), head_narrow[toks : 2 * toks]
    ).astype(jnp.bfloat16)
    loads[0].wait()
    loads[1].wait()

    def project(dest):
        term[dest] = jnp.dot(
            heads[pl.ds(pl.multiple_of(dest * own, own), own), :],
            out_rows[...],
            preferred_element_type=jnp.float32,
        ).astype(jnp.bfloat16)

    def pair_term(place, dest):
        return remote(
            term.at[dest], term_in.at[place], tp_send.at[place], tp_recv.at[place], to_partner
        )

    cross_term = remote(term_sum, term_cross, tp_send.at[2], tp_recv.at[2], to_across)
    project(diagonal)
    pair_term(0, diagonal).start()
    project(across)
    project(partner)
    pair_term(1, partner).start()
    project(me_t)
    pair_term(0, diagonal).wait_recv()
    term_sum[...] = (
        term[across].astype(jnp.float32) + term_in[0].astype(jnp.float32)
    ).astype(jnp.bfloat16)
    cross_term.start()
    pair_term(1, partner).wait_recv()
    state = (
        residual[...].astype(jnp.float32)
        + term[me_t].astype(jnp.float32)
        + term_in[1].astype(jnp.float32)
    )
    cross_term.wait_recv()
    state = (state + term_cross[...].astype(jnp.float32)).astype(jnp.bfloat16)
    attended[...] = state
    state = state.astype(jnp.float32)
    normed = (
        state
        * lax.rsqrt(jnp.mean(state * state, axis=-1, keepdims=True) + EPS)
        * norm_gain[...]
    ).astype(jnp.bfloat16)
    rows_all[me_s, me_t, :, 0:width] = normed
    rows_all[me_s, me_t, :, width : width + LANES] = routed[...]

    def spread(z, t, way, target):
        return remote(
            rows_all.at[z, t], rows_all.at[z, t], ag_send.at[z, way], ag_recv.at[z, t], target
        )

    spread(me_s, me_t, 2, to_across).start()

    @pl.when(has_right)
    def _():
        spread(me_s, me_t, 0, to_right).start()

    @pl.when(has_left)
    def _():
        spread(me_s, me_t, 1, to_left).start()

    spread(me_s, me_t, 3, to_partner).start()
    for load in loads[2:]:
        load.wait()

    def pair_part(z, side, dest):
        return remote(
            part.at[z, dest],
            pair_in.at[z, side],
            pair_send.at[z, side],
            pair_recv.at[z, side],
            to_partner,
        )

    def cross_part(z, h):
        return remote(
            pair_sum.at[z, h],
            cross_in.at[z, h],
            cross_send.at[z, h],
            cross_recv.at[z, h],
            to_across,
        )

    def cross_start(z, h):
        pair_sum[z, h] = (
            part[z, across, h].astype(jnp.float32) + pair_in[z, 0, h].astype(jnp.float32)
        ).astype(jnp.bfloat16)
        cross_part(z, h).start()

    lane = lane_index((group, LANES))
    mine = (lane < 3 * n_sp) & (lane % n_sp == me_s)

    def expert_step(i, carry):
        z = pick(near, me_s, i)
        lower, upper = me_s - (i + 1), me_s + (i + 1)

        @pl.when(lower >= 0)
        def _():
            spread(lower, me_t, 0, to_right).wait_recv()

            @pl.when(has_right)
            def _():
                spread(lower, me_t, 0, to_right).start()

            spread(lower, me_t, 2, to_across).start()
            spread(lower, me_t, 3, to_partner).start()

        @pl.when(upper < n_sp)
        def _():
            spread(upper, me_t, 1, to_left).wait_recv()

            @pl.when(has_left)
            def _():
                spread(upper, me_t, 1, to_left).start()

            spread(upper, me_t, 2, to_across).start()
            spread(upper, me_t, 3, to_partner).start()

        spread(z, across, 4, to_partner).wait_recv()
        spread(z, across, 4, to_partner).start()
        spread(z, partner, 3, to_partner).wait_recv()
        spread(z, diagonal, 3, to_partner).wait_recv()

        @pl.when(i == n_sp - 1)
        def _():
            pair_part(me_s, 0, diagonal).wait_recv()
            for h in range(2):
                cross_start(me_s, h)

        weight = jnp.sum(
            jnp.where(
                mine,
                rows_all[z, :, :, width : width + LANES]
                .astype(jnp.float32)
                .reshape(group, LANES),
                0.0,
            ),
            axis=-1,
            keepdims=True,
        )
        inputs = rows_all[z, :, :, 0:width].reshape(group, width)
        for j in range(chunks):
            act = jnp.dot(
                inputs,
                gate_up[:, 2 * j * LANES : 2 * (j + 1) * LANES],
                preferred_element_type=jnp.float32,
            )
            gate_act, up_act = act[:, 0:LANES], act[:, LANES : 2 * LANES]
            hidden[:, j * LANES : (j + 1) * LANES] = (
                gate_act / (1.0 + jnp.exp(-gate_act)) * up_act
            ).astype(jnp.bfloat16)
        for j in range(width // (2 * LANES)):
            piece = jnp.dot(
                hidden[...],
                down[:, 2 * j * LANES : 2 * (j + 1) * LANES],
                preferred_element_type=jnp.float32,
            )
            side = j // (half // (2 * LANES))
            start = 2 * j * LANES - side * half
            part[z, :, side, :, start : start + 2 * LANES] = (
                (piece * weight).astype(jnp.bfloat16).reshape(n_tp, own, 2 * LANES)
            )
        pair_part(z, 0, diagonal).start()
        pair_part(z, 1, partner).start()
        return carry

    lax.fori_loop(0, n_sp, expert_step, 0)

    def cross_step(i, carry):
        z = pick(far, me_s, i)
        pair_part(z, 0, diagonal).wait_recv()
        for h in range(2):
            cross_start(z, h)
        return carry

    lax.fori_loop(0, n_sp - 1, cross_step, 0)

    def chain_copy(z, slot, h, target):
        return remote(
            chain_out.at[z, h],
            chain_in.at[slot, h],
            chain_send.at[z, h],
            chain_recv.at[slot, h],
            target,
        )

    def gathered(z, h):
        cross_part(z, h).wait_recv()
        return (
            part[z, me_t, h].astype(jnp.float32)
            + pair_in[z, 1, h].astype(jnp.float32)
            + cross_in[z, h].astype(jnp.float32)
        )

    def chain_step(i, carry):
        z, h = pick(far, me_s, i // 2), i % 2
        chain_in_here = jnp.where(z > me_s, me_s, n_sp - 1 - me_s) > 0

        @pl.when(h == 0)
        def _():
            pair_part(z, 1, partner).wait_recv()

        chain_out[z, h] = gathered(z, h).astype(jnp.bfloat16)

        @pl.when(chain_in_here)
        def _():
            chain_copy(z, z, h, to_right).wait_recv()
            chain_out[z, h] = (
                chain_out[z, h].astype(jnp.float32) + chain_in[z, h].astype(jnp.float32)
            ).astype(jnp.bfloat16)

        @pl.when(z > me_s)
        def _():
            chain_copy(z, z, h, to_right).start()

        @pl.when(z < me_s)
        def _():
            chain_copy(z, jnp.where(z == me_s - 1, n_sp, z), h, to_left).start()

        return carry

    lax.fori_loop(0, 2 * (n_sp - 1), chain_step, 0)

    pair_part(me_s, 1, partner).wait_recv()
    for h in range(2):
        columns = slice(h * half, (h + 1) * half)
        final[...] = attended[:, columns].astype(jnp.float32) + gathered(me_s, h)

        @pl.when(has_left)
        def _():
            chain_copy(me_s, me_s, h, to_right).wait_recv()
            final[...] = final[...] + chain_in[me_s, h].astype(jnp.float32)

        @pl.when(has_right)
        def _():
            chain_copy(me_s, n_sp, h, to_left).wait_recv()
            final[...] = final[...] + chain_in[n_sp, h].astype(jnp.float32)

        result[:, columns] = final[...].astype(jnp.bfloat16)

    pair_term(0, diagonal).wait_send()
    pair_term(1, partner).wait_send()
    cross_term.wait_send()

    def drain(z, carry):
        for h in range(2):
            cross_part(z, h).wait_send()
        pair_part(z, 0, diagonal).wait_send()
        pair_part(z, 1, partner).wait_send()
        spread(z, me_t, 2, to_across).wait_send()
        spread(z, me_t, 3, to_partner).wait_send()
        spread(z, across, 4, to_partner).wait_send()

        @pl.when((z <= me_s) & has_right)
        def _():
            kv_copy(z, 0, to_right).wait_send()
            spread(z, me_t, 0, to_right).wait_send()

        @pl.when((z >= me_s) & has_left)
        def _():
            kv_copy(z, 1, to_left).wait_send()
            spread(z, me_t, 1, to_left).wait_send()

        @pl.when(z != me_s)
        def _():
            for h in range(2):
                chain_copy(z, z, h, to_right).wait_send()

        return carry

    lax.fori_loop(0, n_sp, drain, 0)


def signed_tables(tok_count, head_width):
    places = np.arange(tok_count, dtype=np.int32)
    quarter = head_width // 4
    inv_freq = np.float32(THETA) ** (-np.arange(quarter, dtype=np.float32) / np.float32(quarter))
    row_angle = (places // GRID).astype(np.float32)[:, None] * inv_freq[None, :]
    col_angle = (places % GRID).astype(np.float32)[:, None] * inv_freq[None, :]
    angles = np.concatenate([row_angle, row_angle, col_angle, col_angle], axis=-1)
    sign = np.where(np.arange(head_width) % (2 * quarter) < quarter, -1.0, 1.0)
    cos_table, sin_table = np.cos(angles), np.sin(angles) * sign.astype(np.float32)
    copies = LANES // head_width
    return [np.tile(table, (1, copies)).astype(np.float32) for table in (cos_table, sin_table)]


def fused_body(
    residual,
    queries_wide,
    keys_wide,
    values_wide,
    queries_narrow,
    keys_narrow,
    values_narrow,
    query_gain_wide,
    key_gain_wide,
    query_gain_narrow,
    key_gain_narrow,
    output_wide,
    output_narrow,
    norm_gain,
    gate_weight,
    up_weight,
    down_weight,
    route_ids,
    route_weights,
):
    n_sp, n_tp = lax.axis_size("sp"), lax.axis_size("tp")
    own, width = residual.shape
    toks = queries_wide.shape[0]
    half = width // 2
    units = gate_weight.shape[2]
    whole = n_sp * toks
    tables = np.stack(
        signed_tables(whole, query_gain_wide.shape[0])
        + signed_tables(whole, query_gain_narrow.shape[0])
    )
    tables = jnp.asarray(tables.reshape(4, n_sp, toks, LANES))
    lane = jnp.arange(LANES, dtype=jnp.int32)[None, :]
    dense = jnp.zeros((own, LANES), jnp.float32)
    for k in range(route_ids.shape[1]):
        dense += jnp.where(route_ids[:, k : k + 1] == lane % n_sp, route_weights[:, k : k + 1], 0.0)
    first = lax.reduce_precision(dense, 8, 7)
    second = lax.reduce_precision(dense - first, 8, 7)
    third = dense - first - second
    routed = jnp.where(lane < n_sp, first, jnp.where(lane < 2 * n_sp, second, third))
    routed = jnp.where(lane < 3 * n_sp, routed, 0.0).astype(jnp.bfloat16)
    vmem = pl.BlockSpec(memory_space=pltpu.VMEM)
    anywhere = pl.BlockSpec(memory_space=pl.ANY)
    low_type, full_type = jnp.bfloat16, jnp.float32
    dma = pltpu.SemaphoreType.DMA
    scratch = [
        pltpu.VMEM((n_sp, toks, 3 * LANES), low_type),
        pltpu.VMEM((2 * toks, LANES), low_type),
        pltpu.VMEM((2 * toks, LANES), low_type),
        pltpu.VMEM((2, 2 * toks, 1), full_type),
        pltpu.VMEM((2, 2 * toks, 1), full_type),
        pltpu.VMEM((2, 2 * toks, LANES), full_type),
        pltpu.VMEM((toks, 3 * LANES), low_type),
        pltpu.VMEM((3 * LANES, width), low_type),
        pltpu.VMEM((n_tp, own, width), low_type),
        pltpu.VMEM((2, own, width), low_type),
        pltpu.VMEM((own, width), low_type),
        pltpu.VMEM((own, width), low_type),
        pltpu.VMEM((own, width), low_type),
        pltpu.VMEM((n_sp, n_tp, own, width + LANES), low_type),
        pltpu.VMEM((width, 2 * units), low_type),
        pltpu.VMEM((units, width), low_type),
        pltpu.VMEM((n_tp * own, units), low_type),
        pltpu.VMEM((n_sp, n_tp, 2, own, half), low_type),
        pltpu.VMEM((n_sp, 2, 2, own, half), low_type),
        pltpu.VMEM((n_sp, 2, own, half), low_type),
        pltpu.VMEM((n_sp, 2, own, half), low_type),
        pltpu.VMEM((n_sp, 2, own, half), low_type),
        pltpu.VMEM((n_sp + 1, 2, own, half), low_type),
        pltpu.VMEM((own, half), full_type),
        pltpu.VMEM((4, toks, LANES), full_type),
        dma((4 + 2 * (units // LANES),)),
        dma((2, n_sp)),
        dma((n_sp,)),
        dma((3,)),
        dma((3,)),
        dma((n_sp, 5)),
        dma((n_sp, n_tp)),
        dma((n_sp, 2)),
        dma((n_sp, 2)),
        dma((n_sp, 2)),
        dma((n_sp, 2)),
        dma((n_sp, 2)),
        dma((n_sp + 1, 2)),
    ]
    return pl.pallas_call(
        functools.partial(fused_kernel, n_sp, n_tp),
        out_shape=jax.ShapeDtypeStruct(residual.shape, residual.dtype),
        in_specs=[vmem] * 7 + [anywhere] + [vmem] * 6 + [anywhere] * 5,
        out_specs=vmem,
        scratch_shapes=scratch,
        compiler_params=pltpu.CompilerParams(
            collective_id=0, has_side_effects=True, vmem_limit_bytes=60 * 1024 * 1024
        ),
        name="fused_layer",
    )(
        residual,
        queries_wide,
        keys_wide,
        values_wide,
        queries_narrow,
        keys_narrow.T,
        values_narrow.T,
        tables,
        query_gain_wide.reshape(1, LANES),
        key_gain_wide.reshape(1, LANES),
        query_gain_narrow.reshape(1, LANES // 2),
        key_gain_narrow.reshape(1, LANES // 2),
        norm_gain.reshape(1, width),
        routed,
        output_wide,
        output_narrow,
        gate_weight,
        up_weight,
        down_weight,
    )


def body(*operands):
    residual, queries_wide, keys_wide = operands[0], operands[1], operands[2]
    queries_narrow, keys_narrow = operands[4], operands[5]
    wide_width, narrow_width = operands[7].shape[0], operands[9].shape[0]
    n_sp, n_tp = lax.axis_size("sp"), lax.axis_size("tp")
    own = residual.shape[0]
    fits = (
        n_tp == 4
        and 2 <= n_sp <= 8
        and 2 * operands[17].shape[1] * own // n_sp >= own
        and wide_width == LANES
        and narrow_width == LANES // 2
        and queries_wide.shape[1] == 2 * LANES
        and keys_wide.shape[1] == LANES
        and queries_narrow.shape[1] == LANES
        and keys_narrow.shape[1] == LANES // 2
        and queries_wide.shape[0] == n_tp * own
        and own % 16 == 0
    )
    return fused_body(*operands) if fits else plain_body(*operands)


def solution(mesh):
    return jax.shard_map(
        body,
        mesh=mesh,
        in_specs=(
            P(("grp", "sp", "tp"), None),
            P(("grp", "sp"), "tp"),
            P(("grp", "sp"), "tp"),
            P(("grp", "sp"), "tp"),
            P(("grp", "sp"), "tp"),
            P(("grp", "sp"), "tp"),
            P(("grp", "sp"), "tp"),
            P(),
            P(),
            P(),
            P(),
            P("tp", None),
            P("tp", None),
            P(),
            P("sp", None, "tp"),
            P("sp", None, "tp"),
            P("sp", "tp", None),
            P(("grp", "sp", "tp"), None),
            P(("grp", "sp", "tp"), None),
        ),
        out_specs=P(("grp", "sp", "tp"), None),
        check_vma=False,
    )
```

profile of v0, /device:TPU:0, one launch (start us, length us, event | category | flops | bytes accessed | tf_op | source)
XLA Modules:
  0.0 102.1 jit_solution(1609345647873863410)
XLA Ops:
  0.0 0.8 slice_bitcast_fusion.3
  0.8 0.8 slice_bitcast_fusion.2
  1.5 0.7 fusion.1.routed
  2.2 98.2 %fused_layer.1 = bf16[64,2048]{1,0:T(8,128)(2,1)} custom-call(bf16[64,2048]{1,0:T(8,128)(2,1)} %residual.1, bf16[256,256]{1,0:T(8,128)(2,1)} %queries_wide.1, bf16[256,128]{1,0:T(8,128)(2,1)} %keys_wide.1, bf16[256,128]{1,0:T(8,128)(2,1)} %values_wide.1, bf16[256,128]{1,0:T(8,128)(2,1)} %queries_narrow.1, bf16[64,256]{1,0:T(8,128)(2,1)} %bitcast.15, ...), custom_call_target="tpu_custom_call" | custom-call | tf_op jit(solution)/shard_map/fused_layer/pallas_call | solution.py:857
  100.4 1.7 %copy.22 = bf16[64,2048]{1,0:T(8,128)(2,1)} copy(bf16[64,2048]{1,0:T(8,128)(2,1)} %fused_layer.1) | data formatting | bytes 524288
  (3 shorter events, 0.0 us)
where the time goes:
time: 102 us
  Pallas kernels  98.2 us (96%)
  local copies, waits for them, and re-layouts  3.18 us (3%)
    pallas_call x1, Pallas kernels, fused_body(): pl.pallas_call(functools.partial(fused_kernel, n_sp, n_tp), out_shape=jax...  98.2 us

commit v1 on v0

--- a/solution.py
+++ b/solution.py
@@ -217,6 +217,8 @@
 
 LANES = 128
 MESH_IDS = pl.DeviceIdType.MESH
+PIECES = 2
+ORDER = ((0, 1, 2, 3), (1, 0, 3, 2), (2, 3, 0, 1), (3, 2, 1, 0))
 
 
 def pick(table, row, col):
@@ -306,11 +308,14 @@
     hidden,
     part,
     pair_in,
-    pair_sum,
+    cross_out,
     cross_in,
-    chain_out,
-    chain_in,
-    final,
+    single_out,
+    single_in,
+    double_out,
+    double_in,
+    last_out,
+    last_in,
     tables,
     load_sem,
     kv_send,
@@ -323,8 +328,12 @@
     pair_recv,
     cross_send,
     cross_recv,
-    chain_send,
-    chain_recv,
+    single_send,
+    single_recv,
+    double_send,
+    double_recv,
+    last_send,
+    last_recv,
 ):
     me_s = lax.axis_index("sp")
     me_t = lax.axis_index("tp")
@@ -337,7 +346,9 @@
     has_left, has_right = me_s > 0, me_s < n_sp - 1
     to_left, to_right = {"sp": jnp.maximum(me_s - 1, 0)}, {"sp": jnp.minimum(me_s + 1, n_sp - 1)}
     near = [sorted(range(n_sp), key=lambda z: (abs(z - s), z)) for s in range(n_sp)]
-    far = [order[::-1] for order in near]
+    order = ORDER
+    at_end = (me_s == 0) | (me_s == n_sp - 1)
+    to_far = {"sp": jnp.where(me_s == 0, n_sp - 1, 0)}
     own = residual.shape[0]
     width = residual.shape[1]
     toks = queries_wide.shape[0]
@@ -382,6 +393,10 @@
     def _():
         pl.semaphore_signal(barrier, inc=1, device_id=to_right, device_id_type=MESH_IDS)
 
+    @pl.when(at_end)
+    def _():
+        pl.semaphore_signal(barrier, inc=1, device_id=to_far, device_id_type=MESH_IDS)
+
     table_load.wait()
     for load in loads:
         load.start()
@@ -397,7 +412,7 @@
     packed_rot = rotate_half(packed, jnp.concatenate([key_gain_narrow[...]] * 2, axis=1), cos_narrow, sin_narrow)
     kv[me_s, :, 2 * LANES : 3 * LANES] = jnp.where(low, packed_rot, packed).astype(jnp.bfloat16)
 
-    greeted = 2 + jnp.where(has_left, 1, 0) + jnp.where(has_right, 1, 0)
+    greeted = 4
     pl.semaphore_wait(barrier, greeted)
 
     def kv_copy(block, way, target):
@@ -528,23 +543,24 @@
     ).astype(jnp.bfloat16)
     rows_all[me_s, me_t, :, 0:width] = normed
     rows_all[me_s, me_t, :, width : width + LANES] = routed[...]
-
-    def spread(z, t, way, target):
-        return remote(
-            rows_all.at[z, t], rows_all.at[z, t], ag_send.at[z, way], ag_recv.at[z, t], target
-        )
-
-    spread(me_s, me_t, 2, to_across).start()
-
-    @pl.when(has_right)
-    def _():
-        spread(me_s, me_t, 0, to_right).start()
-
-    @pl.when(has_left)
-    def _():
-        spread(me_s, me_t, 1, to_left).start()
-
-    spread(me_s, me_t, 3, to_partner).start()
+    piece_rows = own // PIECES
+
+    def spread(z, t, way, k, target):
+        rows = rows_all.at[z, t, pl.ds(k * piece_rows, piece_rows)]
+        return remote(rows, rows, ag_send.at[z, way, k], ag_recv.at[z, t, k], target)
+
+    for k in range(PIECES):
+        spread(me_s, me_t, 2, k, to_across).start()
+
+        @pl.when(has_right)
+        def _():
+            spread(me_s, me_t, 0, k, to_right).start()
+
+        @pl.when(has_left)
+        def _():
+            spread(me_s, me_t, 1, k, to_left).start()
+
+        spread(me_s, me_t, 3, k, to_partner).start()
     for load in loads[2:]:
         load.wait()
 
@@ -557,73 +573,98 @@
             to_partner,
         )
 
-    def cross_part(z, h):
+    def own_sum(z, h):
+        return part[z, me_t, h].astype(jnp.float32) + pair_in[z, 1, h].astype(jnp.float32)
+
+    def across_sum(z, h):
+        return part[z, across, h].astype(jnp.float32) + pair_in[z, 0, h].astype(jnp.float32)
+
+    def cross_part(z):
+        return remote(cross_out.at[z], cross_in.at[z], cross_send.at[z], cross_recv.at[z], to_across)
+
+    def reach(z):
+        gap = jnp.abs(z - me_s)
+        ahead = z > me_s
+        slot = jnp.where(
+            gap == 2, jnp.where(ahead, 2, 3), jnp.where(ahead == (gap == 1), 0, 1)
+        )
+        return slot, {"sp": jnp.where(gap == 2, (z + me_s) // 2, z)}
+
+    def single(z):
+        slot, target = reach(z)
         return remote(
-            pair_sum.at[z, h],
-            cross_in.at[z, h],
-            cross_send.at[z, h],
-            cross_recv.at[z, h],
-            to_across,
-        )
-
-    def cross_start(z, h):
-        pair_sum[z, h] = (
-            part[z, across, h].astype(jnp.float32) + pair_in[z, 0, h].astype(jnp.float32)
-        ).astype(jnp.bfloat16)
-        cross_part(z, h).start()
-
-    lane = lane_index((group, LANES))
+            single_out.at[z], single_in.at[slot], single_send.at[z], single_recv.at[slot], target
+        )
+
+    def double(z, side):
+        slot, target = reach(z)
+        return remote(
+            double_out.at[z, side],
+            double_in.at[slot, side],
+            double_send.at[z, side],
+            double_recv.at[slot, side],
+            target,
+        )
+
+    def single_arrived(slot):
+        remote(
+            single_out.at[0], single_in.at[slot], single_send.at[0], single_recv.at[slot], to_left
+        ).wait_recv()
+
+    def double_arrived(slot, side):
+        remote(
+            double_out.at[0, side],
+            double_in.at[slot, side],
+            double_send.at[0, side],
+            double_recv.at[slot, side],
+            to_left,
+        ).wait_recv()
+
+    has_mid = has_left & has_right
+
+    def relayed(z):
+        return has_mid & (jnp.abs(z - me_s) == 1)
+
+    def combine_own(z):
+        pair_part(z, 1, partner).wait_recv()
+
+        @pl.when((z != me_s) & jnp.logical_not(relayed(z)))
+        def _():
+            double_out[z, 0] = own_sum(z, 1).astype(jnp.bfloat16)
+            double(z, 0).start()
+
+    def combine_across(z):
+        pair_part(z, 0, diagonal).wait_recv()
+        cross_out[z] = across_sum(z, 0).astype(jnp.bfloat16)
+        cross_part(z).start()
+
+        @pl.when((z != me_s) & jnp.logical_not(relayed(z)))
+        def _():
+            double_out[z, 1] = across_sum(z, 1).astype(jnp.bfloat16)
+            double(z, 1).start()
+
+    def launch(z):
+        @pl.when((z != me_s) & jnp.logical_not(relayed(z)))
+        def _():
+            cross_part(z).wait_recv()
+            single_out[z] = (own_sum(z, 0) + cross_in[z].astype(jnp.float32)).astype(jnp.bfloat16)
+            single(z).start()
+
+    lane = lane_index((2 * own, LANES))
     mine = (lane < 3 * n_sp) & (lane % n_sp == me_s)
 
-    def expert_step(i, carry):
-        z = pick(near, me_s, i)
-        lower, upper = me_s - (i + 1), me_s + (i + 1)
-
-        @pl.when(lower >= 0)
-        def _():
-            spread(lower, me_t, 0, to_right).wait_recv()
-
-            @pl.when(has_right)
-            def _():
-                spread(lower, me_t, 0, to_right).start()
-
-            spread(lower, me_t, 2, to_across).start()
-            spread(lower, me_t, 3, to_partner).start()
-
-        @pl.when(upper < n_sp)
-        def _():
-            spread(upper, me_t, 1, to_left).wait_recv()
-
-            @pl.when(has_left)
-            def _():
-                spread(upper, me_t, 1, to_left).start()
-
-            spread(upper, me_t, 2, to_across).start()
-            spread(upper, me_t, 3, to_partner).start()
-
-        spread(z, across, 4, to_partner).wait_recv()
-        spread(z, across, 4, to_partner).start()
-        spread(z, partner, 3, to_partner).wait_recv()
-        spread(z, diagonal, 3, to_partner).wait_recv()
-
-        @pl.when(i == n_sp - 1)
-        def _():
-            pair_part(me_s, 0, diagonal).wait_recv()
-            for h in range(2):
-                cross_start(me_s, h)
-
+    def expert_half(z, col):
+        rows = rows_all.at[z, pl.ds(2 * col, 2)]
         weight = jnp.sum(
             jnp.where(
                 mine,
-                rows_all[z, :, :, width : width + LANES]
-                .astype(jnp.float32)
-                .reshape(group, LANES),
+                rows[:, :, width : width + LANES].astype(jnp.float32).reshape(2 * own, LANES),
                 0.0,
             ),
             axis=-1,
             keepdims=True,
         )
-        inputs = rows_all[z, :, :, 0:width].reshape(group, width)
+        inputs = rows[:, :, 0:width].reshape(2 * own, width)
         for j in range(chunks):
             act = jnp.dot(
                 inputs,
@@ -642,114 +683,160 @@
             )
             side = j // (half // (2 * LANES))
             start = 2 * j * LANES - side * half
-            part[z, :, side, :, start : start + 2 * LANES] = (
-                (piece * weight).astype(jnp.bfloat16).reshape(n_tp, own, 2 * LANES)
+            part[z, pl.ds(2 * col, 2), side, :, start : start + 2 * LANES] = (
+                (piece * weight).astype(jnp.bfloat16).reshape(2, own, 2 * LANES)
             )
-        pair_part(z, 0, diagonal).start()
-        pair_part(z, 1, partner).start()
+
+    def expert_step(step, carry):
+        i, k = step // 2, step % 2
+        z = pick(order, me_s, i)
+        lower, upper = me_s - (i + 1), me_s + (i + 1)
+
+        @pl.when(lower >= 0)
+        def _():
+            spread(lower, me_t, 0, k, to_right).wait_recv()
+
+            @pl.when(has_right)
+            def _():
+                spread(lower, me_t, 0, k, to_right).start()
+
+            spread(lower, me_t, 3, k, to_partner).start()
+
+        @pl.when(upper < n_sp)
+        def _():
+            spread(upper, me_t, 1, k, to_left).wait_recv()
+
+            @pl.when(has_left)
+            def _():
+                spread(upper, me_t, 1, k, to_left).start()
+
+            spread(upper, me_t, 3, k, to_partner).start()
+
+        @pl.when(i < n_sp - 1)
+        def _():
+            spread(pick(order, me_s, jnp.minimum(i + 1, n_sp - 1)), me_t, 2, k, to_across).start()
+
+        spread(z, across, 4, k, to_partner).wait_recv()
+        spread(z, across, 4, k, to_partner).start()
+
+        @pl.when(k == 0)
+        def _():
+            for p in range(PIECES):
+                spread(z, partner, 3, p, to_partner).wait_recv()
+
+        @pl.when(k == 1)
+        def _():
+            combine_own(z)
+
+            @pl.when(i >= 2)
+            def _():
+                combine_across(pick(order, me_s, i - 1))
+
+        @pl.when(k == 1)
+        def _():
+            for p in range(PIECES):
+                spread(z, diagonal, 3, p, to_partner).wait_recv()
+
+        expert_half(z, jnp.where(k == 0, column, 1 - column))
+        pair_part(z, 1 - k, jnp.where(k == 0, partner, diagonal)).start()
         return carry
 
-    lax.fori_loop(0, n_sp, expert_step, 0)
-
-    def cross_step(i, carry):
-        z = pick(far, me_s, i)
-        pair_part(z, 0, diagonal).wait_recv()
-        for h in range(2):
-            cross_start(z, h)
-        return carry
-
-    lax.fori_loop(0, n_sp - 1, cross_step, 0)
-
-    def chain_copy(z, slot, h, target):
-        return remote(
-            chain_out.at[z, h],
-            chain_in.at[slot, h],
-            chain_send.at[z, h],
-            chain_recv.at[slot, h],
-            target,
-        )
-
-    def gathered(z, h):
-        cross_part(z, h).wait_recv()
-        return (
-            part[z, me_t, h].astype(jnp.float32)
-            + pair_in[z, 1, h].astype(jnp.float32)
-            + cross_in[z, h].astype(jnp.float32)
-        )
-
-    def chain_step(i, carry):
-        z, h = pick(far, me_s, i // 2), i % 2
-        chain_in_here = jnp.where(z > me_s, me_s, n_sp - 1 - me_s) > 0
-
-        @pl.when(h == 0)
-        def _():
-            pair_part(z, 1, partner).wait_recv()
-
-        chain_out[z, h] = gathered(z, h).astype(jnp.bfloat16)
-
-        @pl.when(chain_in_here)
-        def _():
-            chain_copy(z, z, h, to_right).wait_recv()
-            chain_out[z, h] = (
-                chain_out[z, h].astype(jnp.float32) + chain_in[z, h].astype(jnp.float32)
-            ).astype(jnp.bfloat16)
-
-        @pl.when(z > me_s)
-        def _():
-            chain_copy(z, z, h, to_right).start()
-
-        @pl.when(z < me_s)
-        def _():
-            chain_copy(z, jnp.where(z == me_s - 1, n_sp, z), h, to_left).start()
-
-        return carry
-
-    lax.fori_loop(0, 2 * (n_sp - 1), chain_step, 0)
-
-    pair_part(me_s, 1, partner).wait_recv()
-    for h in range(2):
-        columns = slice(h * half, (h + 1) * half)
-        final[...] = attended[:, columns].astype(jnp.float32) + gathered(me_s, h)
-
-        @pl.when(has_left)
-        def _():
-            chain_copy(me_s, me_s, h, to_right).wait_recv()
-            final[...] = final[...] + chain_in[me_s, h].astype(jnp.float32)
-
-        @pl.when(has_right)
-        def _():
-            chain_copy(me_s, n_sp, h, to_left).wait_recv()
-            final[...] = final[...] + chain_in[n_sp, h].astype(jnp.float32)
-
-        result[:, columns] = final[...].astype(jnp.bfloat16)
+    lax.fori_loop(0, 2 * n_sp, expert_step, 0)
+    launch(pick(order, me_s, 1))
+    combine_across(pick(order, me_s, n_sp - 1))
+    combine_across(me_s)
+    launch(pick(order, me_s, n_sp - 2))
+    def pass_double(z, slot):
+        double_arrived(slot, 0)
+        double_out[z, 0] = (own_sum(z, 1) + double_in[slot, 0].astype(jnp.float32)).astype(
+            jnp.bfloat16
+        )
+        double(z, 0).start()
+        double_arrived(slot, 1)
+        double_out[z, 1] = (across_sum(z, 1) + double_in[slot, 1].astype(jnp.float32)).astype(
+            jnp.bfloat16
+        )
+        double(z, 1).start()
+
+    def pass_single(z, slot):
+        cross_part(z).wait_recv()
+        single_arrived(slot)
+        single_out[z] = (
+            own_sum(z, 0)
+            + cross_in[z].astype(jnp.float32)
+            + single_in[slot].astype(jnp.float32)
+        ).astype(jnp.bfloat16)
+        single(z).start()
+
+    @pl.when(has_mid)
+    def _():
+        for z, slot in ((me_s + 1, 2), (me_s - 1, 3)):
+            pass_double(z, slot)
+        for z, slot in ((me_s + 1, 2), (me_s - 1, 3)):
+            pass_single(z, slot)
+
+    launch(pick(order, me_s, n_sp - 1))
+
+    last_cross = remote(last_out, last_in, last_send.at[0], last_recv.at[0], to_across)
+    for slot in range(2):
+        for side in range(2):
+            double_arrived(slot, side)
+    last_out[...] = (
+        across_sum(me_s, 1)
+        + double_in[0, 1].astype(jnp.float32)
+        + double_in[1, 1].astype(jnp.float32)
+    ).astype(jnp.bfloat16)
+    last_cross.start()
+    cross_part(me_s).wait_recv()
+    single_arrived(0)
+    single_arrived(1)
+    result[:, 0:half] = (
+        attended[:, 0:half].astype(jnp.float32)
+        + own_sum(me_s, 0)
+        + cross_in[me_s].astype(jnp.float32)
+        + single_in[0].astype(jnp.float32)
+        + single_in[1].astype(jnp.float32)
+    ).astype(jnp.bfloat16)
+    partial = (
+        attended[:, half:width].astype(jnp.float32)
+        + own_sum(me_s, 1)
+        + double_in[0, 0].astype(jnp.float32)
+        + double_in[1, 0].astype(jnp.float32)
+    )
+    last_cross.wait_recv()
+    result[:, half:width] = (partial + last_in[...].astype(jnp.float32)).astype(jnp.bfloat16)
 
     pair_term(0, diagonal).wait_send()
     pair_term(1, partner).wait_send()
     cross_term.wait_send()
+    last_cross.wait_send()
 
     def drain(z, carry):
-        for h in range(2):
-            cross_part(z, h).wait_send()
+        cross_part(z).wait_send()
         pair_part(z, 0, diagonal).wait_send()
         pair_part(z, 1, partner).wait_send()
-        spread(z, me_t, 2, to_across).wait_send()
-        spread(z, me_t, 3, to_partner).wait_send()
-        spread(z, across, 4, to_partner).wait_send()
+        for k in range(PIECES):
+            spread(z, me_t, 2, k, to_across).wait_send()
+            spread(z, me_t, 3, k, to_partner).wait_send()
+            spread(z, across, 4, k, to_partner).wait_send()
 
         @pl.when((z <= me_s) & has_right)
         def _():
             kv_copy(z, 0, to_right).wait_send()
-            spread(z, me_t, 0, to_right).wait_send()
+            for k in range(PIECES):
+                spread(z, me_t, 0, k, to_right).wait_send()
 
         @pl.when((z >= me_s) & has_left)
         def _():
             kv_copy(z, 1, to_left).wait_send()
-            spread(z, me_t, 1, to_left).wait_send()
+            for k in range(PIECES):
+                spread(z, me_t, 1, k, to_left).wait_send()
 
         @pl.when(z != me_s)
         def _():
-            for h in range(2):
-                chain_copy(z, z, h, to_right).wait_send()
+            single(z).wait_send()
+            double(z, 0).wait_send()
+            double(z, 1).wait_send()
 
         return carry
 
@@ -831,28 +918,35 @@
         pltpu.VMEM((n_sp, n_tp, own, width + LANES), low_type),
         pltpu.VMEM((width, 2 * units), low_type),
         pltpu.VMEM((units, width), low_type),
-        pltpu.VMEM((n_tp * own, units), low_type),
+        pltpu.VMEM((2 * own, units), low_type),
         pltpu.VMEM((n_sp, n_tp, 2, own, half), low_type),
         pltpu.VMEM((n_sp, 2, 2, own, half), low_type),
+        pltpu.VMEM((n_sp, own, half), low_type),
+        pltpu.VMEM((n_sp, own, half), low_type),
+        pltpu.VMEM((n_sp, own, half), low_type),
+        pltpu.VMEM((4, own, half), low_type),
         pltpu.VMEM((n_sp, 2, own, half), low_type),
-        pltpu.VMEM((n_sp, 2, own, half), low_type),
-        pltpu.VMEM((n_sp, 2, own, half), low_type),
-        pltpu.VMEM((n_sp + 1, 2, own, half), low_type),
-        pltpu.VMEM((own, half), full_type),
+        pltpu.VMEM((4, 2, own, half), low_type),
+        pltpu.VMEM((own, half), low_type),
+        pltpu.VMEM((own, half), low_type),
         pltpu.VMEM((4, toks, LANES), full_type),
         dma((4 + 2 * (units // LANES),)),
         dma((2, n_sp)),
         dma((n_sp,)),
         dma((3,)),
         dma((3,)),
-        dma((n_sp, 5)),
-        dma((n_sp, n_tp)),
+        dma((n_sp, 5, PIECES)),
+        dma((n_sp, n_tp, PIECES)),
         dma((n_sp, 2)),
         dma((n_sp, 2)),
+        dma((n_sp,)),
+        dma((n_sp,)),
+        dma((n_sp,)),
+        dma((4,)),
         dma((n_sp, 2)),
-        dma((n_sp, 2)),
-        dma((n_sp, 2)),
-        dma((n_sp + 1, 2)),
+        dma((4, 2)),
+        dma((1,)),
+        dma((1,)),
     ]
     return pl.pallas_call(
         functools.partial(fused_kernel, n_sp, n_tp),
@@ -895,7 +989,7 @@
     own = residual.shape[0]
     fits = (
         n_tp == 4
-        and 2 <= n_sp <= 8
+        and n_sp == len(ORDER)
         and 2 * operands[17].shape[1] * own // n_sp >= own
         and wide_width == LANES
         and narrow_width == LANES // 2
@@ -904,7 +998,7 @@
         and queries_narrow.shape[1] == LANES
         and keys_narrow.shape[1] == LANES // 2
         and queries_wide.shape[0] == n_tp * own
-        and own % 16 == 0
+        and own % (16 * PIECES) == 0
     )
     return fused_body(*operands) if fits else plain_body(*operands)
 

time: 102 us -> 93.3 us (0.915)
  Pallas kernels: 98.2 us -> 89.1 us
    pallas_call x1, Pallas kernels: 98.2 us -> 89.1 us  [fused_body(): pl.pallas_call(functools.partial(fused_kernel, n_sp, n_tp), out_shape=jax...]
where the time goes in v1:
time: 93.3 us; the launch traced here: 93.1 us
  Pallas kernels  89.1 us (95%)
  local copies, waits for them, and re-layouts  3.18 us (3%)
    pallas_call x1, Pallas kernels, fused_body(): pl.pallas_call(functools.partial(fused_kernel, n_sp, n_tp), out_shape=jax...  89.1 us

profile of v1, /device:TPU:0, one launch (start us, length us, event | category | flops | bytes accessed | tf_op | source)
XLA Modules:
  0.0 93.1 jit_solution(13568667966743704478)
XLA Ops:
  0.0 0.8 slice_bitcast_fusion.3
  0.8 0.8 slice_bitcast_fusion.2
  1.5 0.7 fusion.1.routed
  2.2 89.1 %fused_layer.1 = bf16[64,2048]{1,0:T(8,128)(2,1)} custom-call(bf16[64,2048]{1,0:T(8,128)(2,1)} %residual.1, bf16[256,256]{1,0:T(8,128)(2,1)} %queries_wide.1, bf16[256,128]{1,0:T(8,128)(2,1)} %keys_wide.1, bf16[256,128]{1,0:T(8,128)(2,1)} %values_wide.1, bf16[256,128]{1,0:T(8,128)(2,1)} %queries_narrow.1, bf16[64,256]{1,0:T(8,128)(2,1)} %bitcast.15, ...), custom_call_target="tpu_custom_call" | custom-call | tf_op jit(solution)/shard_map/fused_layer/pallas_call | solution.py:951
  91.4 1.7 %copy.22 = bf16[64,2048]{1,0:T(8,128)(2,1)} copy(bf16[64,2048]{1,0:T(8,128)(2,1)} %fused_layer.1) | data formatting | bytes 524288
  (3 shorter events, 0.0 us)

commit v2 on v1

--- a/solution.py
+++ b/solution.py
@@ -218,6 +218,7 @@
 LANES = 128
 MESH_IDS = pl.DeviceIdType.MESH
 PIECES = 2
+LEAD_PARTS = 4
 ORDER = ((0, 1, 2, 3), (1, 0, 3, 2), (2, 3, 0, 1), (3, 2, 1, 0))
 
 
@@ -282,7 +283,8 @@
     query_gain_narrow,
     key_gain_narrow,
     norm_gain,
-    routed,
+    route_ids,
+    route_weights,
     output_wide,
     output_narrow,
     gate_weight,
@@ -317,9 +319,14 @@
     last_out,
     last_in,
     tables,
+    weights,
     load_sem,
     kv_send,
     kv_recv,
+    share_send,
+    share_recv,
+    spread_send,
+    spread_recv,
     tp_send,
     tp_recv,
     ag_send,
@@ -353,7 +360,8 @@
     width = residual.shape[1]
     toks = queries_wide.shape[0]
     group = n_tp * own
-    half = width // 2
+    split = width * LEAD_PARTS // 8
+    n_experts = weights.shape[2]
 
     chunks = gate_weight.shape[2] // LANES
     table_load = pltpu.make_async_copy(
@@ -397,6 +405,42 @@
     def _():
         pl.semaphore_signal(barrier, inc=1, device_id=to_far, device_id_type=MESH_IDS)
 
+    kv[me_s, 0] = values_wide[...]
+    expert = lax.broadcasted_iota(jnp.int32, (n_experts, own), 0)
+    shares = jnp.zeros((n_experts, own), jnp.float32)
+    for k in range(route_ids.shape[0]):
+        shares += jnp.where(route_ids[k : k + 1, :] == expert, route_weights[k : k + 1, :], 0.0)
+    weights[me_s, me_t] = jnp.concatenate([shares, jnp.zeros_like(shares)], axis=1)
+    pl.semaphore_wait(barrier, 4)
+
+    def kv_copy(block, p, way, target):
+        return remote(
+            kv.at[block, p],
+            kv.at[block, p],
+            kv_send.at[way, block, p],
+            kv_recv.at[block, p],
+            target,
+        )
+
+    def share_copy(block, way, target):
+        return remote(
+            weights.at[block, me_t],
+            weights.at[block, me_t],
+            share_send.at[way, block],
+            share_recv.at[block],
+            target,
+        )
+
+    def send_kv(p):
+        @pl.when(has_right)
+        def _():
+            kv_copy(me_s, p, 0, to_right).start()
+
+        @pl.when(has_left)
+        def _():
+            kv_copy(me_s, p, 1, to_left).start()
+
+    send_kv(0)
     table_load.wait()
     for load in loads:
         load.start()
@@ -404,27 +448,22 @@
     cos_narrow, sin_narrow = tables[2], tables[3]
     low = lane_index((toks, LANES)) < LANES // 2
     key_rot = rotate_full(keys_wide[...].astype(jnp.float32), key_gain_wide[...], cos_wide, sin_wide)
-    kv[me_s, :, 0:LANES] = key_rot.astype(jnp.bfloat16)
-    kv[me_s, :, LANES : 2 * LANES] = values_wide[...]
+    kv[me_s, 1] = key_rot.astype(jnp.bfloat16)
+    send_kv(1)
     packed = jnp.concatenate(
         [keys_narrow[...].astype(jnp.float32), values_narrow[...].astype(jnp.float32)], axis=0
     ).T
     packed_rot = rotate_half(packed, jnp.concatenate([key_gain_narrow[...]] * 2, axis=1), cos_narrow, sin_narrow)
-    kv[me_s, :, 2 * LANES : 3 * LANES] = jnp.where(low, packed_rot, packed).astype(jnp.bfloat16)
-
-    greeted = 4
-    pl.semaphore_wait(barrier, greeted)
-
-    def kv_copy(block, way, target):
-        return remote(kv.at[block], kv.at[block], kv_send.at[way, block], kv_recv.at[block], target)
+    kv[me_s, 2] = jnp.where(low, packed_rot, packed).astype(jnp.bfloat16)
+    send_kv(2)
 
     @pl.when(has_right)
     def _():
-        kv_copy(me_s, 0, to_right).start()
+        share_copy(me_s, 0, to_right).start()
 
     @pl.when(has_left)
     def _():
-        kv_copy(me_s, 1, to_left).start()
+        share_copy(me_s, 1, to_left).start()
 
     for h in range(2):
         turned = rotate_full(
@@ -459,38 +498,67 @@
         )
         top[kind] = new_top
 
+    def attend_wide(block):
+        sweep(0, q_wide[...], kv[block, 1], kv[block, 0], LANES**-0.5)
+
+    def attend_narrow(block):
+        both = kv[block, 2]
+        sweep(1, q_narrow[...], both, both, (LANES // 2) ** -0.5)
+
+    attend_wide(me_s)
+    attend_narrow(me_s)
+
     def attend_step(i, carry):
         block = pick(near, me_s, i)
-        sweep(
-            0,
-            q_wide[...],
-            kv[block, :, 0:LANES],
-            kv[block, :, LANES : 2 * LANES],
-            LANES**-0.5,
-        )
-        both = kv[block, :, 2 * LANES : 3 * LANES]
-        sweep(1, q_narrow[...], both, both, (LANES // 2) ** -0.5)
-        lower, upper = me_s - (i + 1), me_s + (i + 1)
+        lower, upper = me_s - i, me_s + i
+
+        def kv_pass(p):
+            @pl.when(lower >= 0)
+            def _():
+                kv_copy(lower, p, 0, to_right).wait_recv()
+
+                @pl.when(has_right)
+                def _():
+                    kv_copy(lower, p, 0, to_right).start()
+
+            @pl.when(upper < n_sp)
+            def _():
+                kv_copy(upper, p, 1, to_left).wait_recv()
+
+                @pl.when(has_left)
+                def _():
+                    kv_copy(upper, p, 1, to_left).start()
+
+        kv_pass(0)
+        kv_pass(1)
+        attend_wide(block)
+        kv_pass(2)
+        attend_narrow(block)
 
         @pl.when(lower >= 0)
         def _():
-            kv_copy(lower, 0, to_right).wait_recv()
+            share_copy(lower, 0, to_right).wait_recv()
 
             @pl.when(has_right)
             def _():
-                kv_copy(lower, 0, to_right).start()
+                share_copy(lower, 0, to_right).start()
 
         @pl.when(upper < n_sp)
         def _():
-            kv_copy(upper, 1, to_left).wait_recv()
+            share_copy(upper, 1, to_left).wait_recv()
 
             @pl.when(has_left)
             def _():
-                kv_copy(upper, 1, to_left).start()
+                share_copy(upper, 1, to_left).start()
 
         return carry
 
-    lax.fori_loop(0, n_sp, attend_step, 0)
+    lax.fori_loop(1, n_sp, attend_step, 0)
+
+    def share_spread(t, way, target):
+        return remote(
+            weights.at[:, t], weights.at[:, t], spread_send.at[way], spread_recv.at[t], target
+        )
 
     head_wide = mixed[0] / total[0]
     head_narrow = mixed[1] / total[1]
@@ -502,54 +570,72 @@
     loads[0].wait()
     loads[1].wait()
 
-    def project(dest):
-        term[dest] = jnp.dot(
-            heads[pl.ds(pl.multiple_of(dest * own, own), own), :],
-            out_rows[...],
-            preferred_element_type=jnp.float32,
+    piece_rows = own // PIECES
+
+    def project(col):
+        place = pl.ds(pl.multiple_of(2 * col * own, 2 * own), 2 * own)
+        term[pl.ds(2 * col, 2)] = (
+            jnp.dot(heads[place, :], out_rows[...], preferred_element_type=jnp.float32)
+            .astype(jnp.bfloat16)
+            .reshape(2, own, width)
+        )
+
+    def rows_of(k):
+        return pl.ds(k * piece_rows, piece_rows)
+
+    def pair_term(place, dest, k):
+        return remote(
+            term.at[dest, rows_of(k)],
+            term_in.at[place, rows_of(k)],
+            tp_send.at[place, k],
+            tp_recv.at[place, k],
+            to_partner,
+        )
+
+    def cross_term(k):
+        return remote(
+            term_sum.at[rows_of(k)],
+            term_cross.at[rows_of(k)],
+            tp_send.at[2, k],
+            tp_recv.at[2, k],
+            to_across,
+        )
+
+    project(1 - column)
+    for k in range(PIECES):
+        pair_term(0, diagonal, k).start()
+    project(column)
+    for k in range(PIECES):
+        pair_term(1, partner, k).start()
+    for k in range(PIECES):
+        pair_term(0, diagonal, k).wait_recv()
+        term_sum[rows_of(k)] = (
+            term[across, rows_of(k)].astype(jnp.float32)
+            + term_in[0, rows_of(k)].astype(jnp.float32)
         ).astype(jnp.bfloat16)
-
-    def pair_term(place, dest):
-        return remote(
-            term.at[dest], term_in.at[place], tp_send.at[place], tp_recv.at[place], to_partner
-        )
-
-    cross_term = remote(term_sum, term_cross, tp_send.at[2], tp_recv.at[2], to_across)
-    project(diagonal)
-    pair_term(0, diagonal).start()
-    project(across)
-    project(partner)
-    pair_term(1, partner).start()
-    project(me_t)
-    pair_term(0, diagonal).wait_recv()
-    term_sum[...] = (
-        term[across].astype(jnp.float32) + term_in[0].astype(jnp.float32)
-    ).astype(jnp.bfloat16)
-    cross_term.start()
-    pair_term(1, partner).wait_recv()
-    state = (
-        residual[...].astype(jnp.float32)
-        + term[me_t].astype(jnp.float32)
-        + term_in[1].astype(jnp.float32)
-    )
-    cross_term.wait_recv()
-    state = (state + term_cross[...].astype(jnp.float32)).astype(jnp.bfloat16)
-    attended[...] = state
-    state = state.astype(jnp.float32)
-    normed = (
-        state
-        * lax.rsqrt(jnp.mean(state * state, axis=-1, keepdims=True) + EPS)
-        * norm_gain[...]
-    ).astype(jnp.bfloat16)
-    rows_all[me_s, me_t, :, 0:width] = normed
-    rows_all[me_s, me_t, :, width : width + LANES] = routed[...]
-    piece_rows = own // PIECES
-
+        cross_term(k).start()
+    share_spread(me_t, 0, to_across).start()
+    share_spread(me_t, 1, to_partner).start()
     def spread(z, t, way, k, target):
-        rows = rows_all.at[z, t, pl.ds(k * piece_rows, piece_rows)]
+        rows = rows_all.at[z, t, rows_of(k)]
         return remote(rows, rows, ag_send.at[z, way, k], ag_recv.at[z, t, k], target)
 
     for k in range(PIECES):
+        pair_term(1, partner, k).wait_recv()
+        cross_term(k).wait_recv()
+        state = (
+            residual[rows_of(k), :].astype(jnp.float32)
+            + term[me_t, rows_of(k)].astype(jnp.float32)
+            + term_in[1, rows_of(k)].astype(jnp.float32)
+            + term_cross[rows_of(k)].astype(jnp.float32)
+        ).astype(jnp.bfloat16)
+        attended[rows_of(k), :] = state
+        state = state.astype(jnp.float32)
+        rows_all[me_s, me_t, rows_of(k)] = (
+            state
+            * lax.rsqrt(jnp.mean(state * state, axis=-1, keepdims=True) + EPS)
+            * norm_gain[...]
+        ).astype(jnp.bfloat16)
         spread(me_s, me_t, 2, k, to_across).start()
 
         @pl.when(has_right)
@@ -561,6 +647,10 @@
             spread(me_s, me_t, 1, k, to_left).start()
 
         spread(me_s, me_t, 3, k, to_partner).start()
+    share_spread(across, 2, to_partner).wait_recv()
+    share_spread(across, 2, to_partner).start()
+    share_spread(partner, 1, to_partner).wait_recv()
+    share_spread(diagonal, 1, to_partner).wait_recv()
     for load in loads[2:]:
         load.wait()
 
@@ -573,11 +663,18 @@
             to_partner,
         )
 
-    def own_sum(z, h):
-        return part[z, me_t, h].astype(jnp.float32) + pair_in[z, 1, h].astype(jnp.float32)
-
-    def across_sum(z, h):
-        return part[z, across, h].astype(jnp.float32) + pair_in[z, 0, h].astype(jnp.float32)
+    lead = pl.ds(0, split)
+    rest = pl.ds(split, width - split)
+
+    def own_sum(z, columns):
+        return part[z, me_t, :, columns].astype(jnp.float32) + pair_in[z, 1, :, columns].astype(
+            jnp.float32
+        )
+
+    def across_sum(z, columns):
+        return part[z, across, :, columns].astype(jnp.float32) + pair_in[
+            z, 0, :, columns
+        ].astype(jnp.float32)
 
     def cross_part(z):
         return remote(cross_out.at[z], cross_in.at[z], cross_send.at[z], cross_recv.at[z], to_across)
@@ -625,46 +722,48 @@
     def relayed(z):
         return has_mid & (jnp.abs(z - me_s) == 1)
 
-    def combine_own(z):
-        pair_part(z, 1, partner).wait_recv()
-
-        @pl.when((z != me_s) & jnp.logical_not(relayed(z)))
-        def _():
-            double_out[z, 0] = own_sum(z, 1).astype(jnp.bfloat16)
-            double(z, 0).start()
-
-    def combine_across(z):
-        pair_part(z, 0, diagonal).wait_recv()
-        cross_out[z] = across_sum(z, 0).astype(jnp.bfloat16)
+    def double_start(z, side):
+        pair_sum = across_sum(z, rest) if side else own_sum(z, rest)
+        double_out[z, side] = pair_sum.astype(jnp.bfloat16)
+        double(z, side).start()
+
+    def double_pass(z, side):
+        slot = jnp.where(z > me_s, 2, 3)
+        double_arrived(slot, side)
+        pair_sum = across_sum(z, rest) if side else own_sum(z, rest)
+        double_out[z, side] = (pair_sum + double_in[slot, side].astype(jnp.float32)).astype(
+            jnp.bfloat16
+        )
+        double(z, side).start()
+
+    def cross_start(z):
+        cross_out[z] = across_sum(z, lead).astype(jnp.bfloat16)
         cross_part(z).start()
 
-        @pl.when((z != me_s) & jnp.logical_not(relayed(z)))
-        def _():
-            double_out[z, 1] = across_sum(z, 1).astype(jnp.bfloat16)
-            double(z, 1).start()
-
-    def launch(z):
-        @pl.when((z != me_s) & jnp.logical_not(relayed(z)))
-        def _():
-            cross_part(z).wait_recv()
-            single_out[z] = (own_sum(z, 0) + cross_in[z].astype(jnp.float32)).astype(jnp.bfloat16)
-            single(z).start()
-
-    lane = lane_index((2 * own, LANES))
-    mine = (lane < 3 * n_sp) & (lane % n_sp == me_s)
+    def single_start(z):
+        cross_part(z).wait_recv()
+        single_out[z] = (own_sum(z, lead) + cross_in[z].astype(jnp.float32)).astype(jnp.bfloat16)
+        single(z).start()
+
+    def single_pass(z):
+        slot = jnp.where(z > me_s, 2, 3)
+        cross_part(z).wait_recv()
+        single_arrived(slot)
+        single_out[z] = (
+            own_sum(z, lead)
+            + cross_in[z].astype(jnp.float32)
+            + single_in[slot].astype(jnp.float32)
+        ).astype(jnp.bfloat16)
+        single(z).start()
 
     def expert_half(z, col):
-        rows = rows_all.at[z, pl.ds(2 * col, 2)]
+        pair = weights.at[z, pl.ds(2 * col, 2)]
+        low_lane = lane_index((n_experts, LANES)) < own
+        by_token = jnp.where(low_lane, pair[0], pltpu.roll(pair[1], LANES - own, 1)).T
         weight = jnp.sum(
-            jnp.where(
-                mine,
-                rows[:, :, width : width + LANES].astype(jnp.float32).reshape(2 * own, LANES),
-                0.0,
-            ),
-            axis=-1,
-            keepdims=True,
-        )
-        inputs = rows[:, :, 0:width].reshape(2 * own, width)
+            jnp.where(lane_index(by_token.shape) == me_s, by_token, 0.0), axis=-1, keepdims=True
+        )
+        inputs = rows_all[z, pl.ds(2 * col, 2)].reshape(2 * own, width)
         for j in range(chunks):
             act = jnp.dot(
                 inputs,
@@ -676,14 +775,9 @@
                 gate_act / (1.0 + jnp.exp(-gate_act)) * up_act
             ).astype(jnp.bfloat16)
         for j in range(width // (2 * LANES)):
-            piece = jnp.dot(
-                hidden[...],
-                down[:, 2 * j * LANES : 2 * (j + 1) * LANES],
-                preferred_element_type=jnp.float32,
-            )
-            side = j // (half // (2 * LANES))
-            start = 2 * j * LANES - side * half
-            part[z, pl.ds(2 * col, 2), side, :, start : start + 2 * LANES] = (
+            columns = slice(2 * j * LANES, 2 * (j + 1) * LANES)
+            piece = jnp.dot(hidden[...], down[:, columns], preferred_element_type=jnp.float32)
+            part[z, pl.ds(2 * col, 2), :, columns] = (
                 (piece * weight).astype(jnp.bfloat16).reshape(2, own, 2 * LANES)
             )
 
@@ -724,13 +818,32 @@
             for p in range(PIECES):
                 spread(z, partner, 3, p, to_partner).wait_recv()
 
+        before = pick(order, me_s, jnp.maximum(i - 1, 0))
+
+        @pl.when((k == 0) & (i >= 2))
+        def _():
+            pair_part(before, 0, diagonal).wait_recv()
+
+            @pl.when(jnp.logical_not(relayed(before)))
+            def _():
+                double_start(before, 1)
+
         @pl.when(k == 1)
         def _():
-            combine_own(z)
+            pair_part(z, 1, partner).wait_recv()
+
+            @pl.when((i >= 1) & jnp.logical_not(relayed(z)))
+            def _():
+                double_start(z, 0)
 
             @pl.when(i >= 2)
             def _():
-                combine_across(pick(order, me_s, i - 1))
+                cross_start(before)
+
+            @pl.when((i == n_sp - 1) & has_mid)
+            def _():
+                double_pass(pick(order, me_s, 1), 0)
+                double_pass(z, 0)
 
         @pl.when(k == 1)
         def _():
@@ -742,47 +855,47 @@
         return carry
 
     lax.fori_loop(0, 2 * n_sp, expert_step, 0)
-    launch(pick(order, me_s, 1))
-    combine_across(pick(order, me_s, n_sp - 1))
-    combine_across(me_s)
-    launch(pick(order, me_s, n_sp - 2))
-    def pass_double(z, slot):
-        double_arrived(slot, 0)
-        double_out[z, 0] = (own_sum(z, 1) + double_in[slot, 0].astype(jnp.float32)).astype(
-            jnp.bfloat16
-        )
-        double(z, 0).start()
-        double_arrived(slot, 1)
-        double_out[z, 1] = (across_sum(z, 1) + double_in[slot, 1].astype(jnp.float32)).astype(
-            jnp.bfloat16
-        )
-        double(z, 1).start()
-
-    def pass_single(z, slot):
-        cross_part(z).wait_recv()
-        single_arrived(slot)
-        single_out[z] = (
-            own_sum(z, 0)
-            + cross_in[z].astype(jnp.float32)
-            + single_in[slot].astype(jnp.float32)
-        ).astype(jnp.bfloat16)
-        single(z).start()
+    first, second, third = (pick(order, me_s, jnp.int32(i)) for i in range(1, n_sp))
+
+    @pl.when(jnp.logical_not(has_mid))
+    def _():
+        single_start(first)
+
+    pair_part(third, 0, diagonal).wait_recv()
+    cross_start(third)
+
+    @pl.when(jnp.logical_not(has_mid))
+    def _():
+        double_start(third, 1)
 
     @pl.when(has_mid)
     def _():
-        for z, slot in ((me_s + 1, 2), (me_s - 1, 3)):
-            pass_double(z, slot)
-        for z, slot in ((me_s + 1, 2), (me_s - 1, 3)):
-            pass_single(z, slot)
-
-    launch(pick(order, me_s, n_sp - 1))
+        double_pass(first, 1)
+
+    single_start(second)
+
+    @pl.when(has_mid)
+    def _():
+        double_pass(third, 1)
+
+    pair_part(me_s, 0, diagonal).wait_recv()
+    cross_start(me_s)
+
+    @pl.when(has_mid)
+    def _():
+        single_pass(first)
+        single_pass(third)
+
+    @pl.when(jnp.logical_not(has_mid))
+    def _():
+        single_start(third)
 
     last_cross = remote(last_out, last_in, last_send.at[0], last_recv.at[0], to_across)
     for slot in range(2):
         for side in range(2):
             double_arrived(slot, side)
     last_out[...] = (
-        across_sum(me_s, 1)
+        across_sum(me_s, rest)
         + double_in[0, 1].astype(jnp.float32)
         + double_in[1, 1].astype(jnp.float32)
     ).astype(jnp.bfloat16)
@@ -790,25 +903,29 @@
     cross_part(me_s).wait_recv()
     single_arrived(0)
     single_arrived(1)
-    result[:, 0:half] = (
-        attended[:, 0:half].astype(jnp.float32)
-        + own_sum(me_s, 0)
+    result[:, lead] = (
+        attended[:, lead].astype(jnp.float32)
+        + own_sum(me_s, lead)
         + cross_in[me_s].astype(jnp.float32)
         + single_in[0].astype(jnp.float32)
         + single_in[1].astype(jnp.float32)
     ).astype(jnp.bfloat16)
     partial = (
-        attended[:, half:width].astype(jnp.float32)
-        + own_sum(me_s, 1)
+        attended[:, rest].astype(jnp.float32)
+        + own_sum(me_s, rest)
         + double_in[0, 0].astype(jnp.float32)
         + double_in[1, 0].astype(jnp.float32)
     )
     last_cross.wait_recv()
-    result[:, half:width] = (partial + last_in[...].astype(jnp.float32)).astype(jnp.bfloat16)
-
-    pair_term(0, diagonal).wait_send()
-    pair_term(1, partner).wait_send()
-    cross_term.wait_send()
+    result[:, rest] = (partial + last_in[...].astype(jnp.float32)).astype(jnp.bfloat16)
+
+    for k in range(PIECES):
+        pair_term(0, diagonal, k).wait_send()
+        pair_term(1, partner, k).wait_send()
+        cross_term(k).wait_send()
+    share_spread(me_t, 0, to_across).wait_send()
+    share_spread(me_t, 1, to_partner).wait_send()
+    share_spread(across, 2, to_partner).wait_send()
     last_cross.wait_send()
 
     def drain(z, carry):
@@ -822,13 +939,17 @@
 
         @pl.when((z <= me_s) & has_right)
         def _():
-            kv_copy(z, 0, to_right).wait_send()
+            for p in range(3):
+                kv_copy(z, p, 0, to_right).wait_send()
+            share_copy(z, 0, to_right).wait_send()
             for k in range(PIECES):
                 spread(z, me_t, 0, k, to_right).wait_send()
 
         @pl.when((z >= me_s) & has_left)
         def _():
-            kv_copy(z, 1, to_left).wait_send()
+            for p in range(3):
+                kv_copy(z, p, 1, to_left).wait_send()
+            share_copy(z, 1, to_left).wait_send()
             for k in range(PIECES):
                 spread(z, me_t, 1, k, to_left).wait_send()
 
@@ -880,7 +1001,7 @@
     n_sp, n_tp = lax.axis_size("sp"), lax.axis_size("tp")
     own, width = residual.shape
     toks = queries_wide.shape[0]
-    half = width // 2
+    split = width * LEAD_PARTS // 8
     units = gate_weight.shape[2]
     whole = n_sp * toks
     tables = np.stack(
@@ -888,21 +1009,12 @@
         + signed_tables(whole, query_gain_narrow.shape[0])
     )
     tables = jnp.asarray(tables.reshape(4, n_sp, toks, LANES))
-    lane = jnp.arange(LANES, dtype=jnp.int32)[None, :]
-    dense = jnp.zeros((own, LANES), jnp.float32)
-    for k in range(route_ids.shape[1]):
-        dense += jnp.where(route_ids[:, k : k + 1] == lane % n_sp, route_weights[:, k : k + 1], 0.0)
-    first = lax.reduce_precision(dense, 8, 7)
-    second = lax.reduce_precision(dense - first, 8, 7)
-    third = dense - first - second
-    routed = jnp.where(lane < n_sp, first, jnp.where(lane < 2 * n_sp, second, third))
-    routed = jnp.where(lane < 3 * n_sp, routed, 0.0).astype(jnp.bfloat16)
     vmem = pl.BlockSpec(memory_space=pltpu.VMEM)
     anywhere = pl.BlockSpec(memory_space=pl.ANY)
     low_type, full_type = jnp.bfloat16, jnp.float32
     dma = pltpu.SemaphoreType.DMA
     scratch = [
-        pltpu.VMEM((n_sp, toks, 3 * LANES), low_type),
+        pltpu.VMEM((n_sp, 3, toks, LANES), low_type),
         pltpu.VMEM((2 * toks, LANES), low_type),
         pltpu.VMEM((2 * toks, LANES), low_type),
         pltpu.VMEM((2, 2 * toks, 1), full_type),
@@ -915,26 +1027,31 @@
         pltpu.VMEM((own, width), low_type),
         pltpu.VMEM((own, width), low_type),
         pltpu.VMEM((own, width), low_type),
-        pltpu.VMEM((n_sp, n_tp, own, width + LANES), low_type),
+        pltpu.VMEM((n_sp, n_tp, own, width), low_type),
         pltpu.VMEM((width, 2 * units), low_type),
         pltpu.VMEM((units, width), low_type),
         pltpu.VMEM((2 * own, units), low_type),
-        pltpu.VMEM((n_sp, n_tp, 2, own, half), low_type),
-        pltpu.VMEM((n_sp, 2, 2, own, half), low_type),
-        pltpu.VMEM((n_sp, own, half), low_type),
-        pltpu.VMEM((n_sp, own, half), low_type),
-        pltpu.VMEM((n_sp, own, half), low_type),
-        pltpu.VMEM((4, own, half), low_type),
-        pltpu.VMEM((n_sp, 2, own, half), low_type),
-        pltpu.VMEM((4, 2, own, half), low_type),
-        pltpu.VMEM((own, half), low_type),
-        pltpu.VMEM((own, half), low_type),
+        pltpu.VMEM((n_sp, n_tp, own, width), low_type),
+        pltpu.VMEM((n_sp, 2, own, width), low_type),
+        pltpu.VMEM((n_sp, own, split), low_type),
+        pltpu.VMEM((n_sp, own, split), low_type),
+        pltpu.VMEM((n_sp, own, split), low_type),
+        pltpu.VMEM((4, own, split), low_type),
+        pltpu.VMEM((n_sp, 2, own, width - split), low_type),
+        pltpu.VMEM((4, 2, own, width - split), low_type),
+        pltpu.VMEM((own, width - split), low_type),
+        pltpu.VMEM((own, width - split), low_type),
         pltpu.VMEM((4, toks, LANES), full_type),
+        pltpu.VMEM((n_sp, n_tp, 8, LANES), full_type),
         dma((4 + 2 * (units // LANES),)),
+        dma((2, n_sp, 3)),
+        dma((n_sp, 3)),
         dma((2, n_sp)),
         dma((n_sp,)),
         dma((3,)),
-        dma((3,)),
+        dma((n_tp,)),
+        dma((3, PIECES)),
+        dma((3, PIECES)),
         dma((n_sp, 5, PIECES)),
         dma((n_sp, n_tp, PIECES)),
         dma((n_sp, 2)),
@@ -951,7 +1068,7 @@
     return pl.pallas_call(
         functools.partial(fused_kernel, n_sp, n_tp),
         out_shape=jax.ShapeDtypeStruct(residual.shape, residual.dtype),
-        in_specs=[vmem] * 7 + [anywhere] + [vmem] * 6 + [anywhere] * 5,
+        in_specs=[vmem] * 7 + [anywhere] + [vmem] * 7 + [anywhere] * 5,
         out_specs=vmem,
         scratch_shapes=scratch,
         compiler_params=pltpu.CompilerParams(
@@ -972,7 +1089,8 @@
         query_gain_narrow.reshape(1, LANES // 2),
         key_gain_narrow.reshape(1, LANES // 2),
         norm_gain.reshape(1, width),
-        routed,
+        route_ids.T,
+        route_weights.T,
         output_wide,
         output_narrow,
         gate_weight,
@@ -990,6 +1108,7 @@
     fits = (
         n_tp == 4
         and n_sp == len(ORDER)
+        and 2 * own == LANES
         and 2 * operands[17].shape[1] * own // n_sp >= own
         and wide_width == LANES
         and narrow_width == LANES // 2

time: 93.3 us -> 82.2 us (0.88)
  Pallas kernels: 89.1 us -> 79.7 us
  local copies, waits for them, and re-layouts: 3.18 us -> 1.67 us
    pallas_call x1, Pallas kernels: 89.1 us -> 79.7 us  [fused_body(): pl.pallas_call(functools.partial(fused_kernel, n_sp, n_tp), out_shape=jax...]
where the time goes in v2:
time: 82.2 us; the launch traced here: 81.3 us
  Pallas kernels  79.7 us (97%)
  local copies, waits for them, and re-layouts  1.67 us (2%)
    pallas_call x1, Pallas kernels, fused_body(): pl.pallas_call(functools.partial(fused_kernel, n_sp, n_tp), out_shape=jax...  79.7 us
    unnamed x1, local copies, waits for them, and re-layouts  1.67 us

profile of v2, /device:TPU:0, one launch (start us, length us, event | category | flops | bytes accessed | tf_op | source)
XLA Modules:
  0.0 81.3 jit_solution(18113464625400665579)
XLA Ops:
  0.0 79.7 %fused_layer.1 = bf16[64,2048]{1,0:T(8,128)(2,1)} custom-call(bf16[64,2048]{1,0:T(8,128)(2,1)} %residual.1, bf16[256,256]{1,0:T(8,128)(2,1)} %queries_wide.1, bf16[256,128]{1,0:T(8,128)(2,1)} %keys_wide.1, bf16[256,128]{1,0:T(8,128)(2,1)} %values_wide.1, bf16[256,128]{1,0:T(8,128)(2,1)} %queries_narrow.1, bf16[64,256]{1,0:T(8,128)(2,1)} %bitcast.9, ...), custom_call_target="tpu_custom_call" | custom-call | tf_op jit(solution)/shard_map/fused_layer/pallas_call | solution.py:1068
  79.7 1.7 %copy.22 = bf16[64,2048]{1,0:T(8,128)(2,1)} copy(bf16[64,2048]{1,0:T(8,128)(2,1)} %fused_layer.1) | data formatting | bytes 524288
